TPU v7x, 32 devices: a whole 2x2x4 slice. The times are simulated.
32 devices in a mesh: ep: 8 (over z, x), tp: 4 (over y, core).
Axes of the slice: x: 2, y: 2, z: 4, core: 2. Of those that a mesh axis runs over, the one named last changes fastest.
Arguments:
- tokens: bfloat16 [192, 3072], P('ep'), may hold values from -6 to 6
- norm_gain: float32 [3072], replicated, may hold values from 0.1 to 1.9
- routing: int32 [192, 4], P('ep'), may hold values from 0 to 7, all different within a row; in each aligned block of 24 rows (0 to 23, 24 to 47, ...) at most 13 rows name the same one
- route_weight: float32 [192, 4], P('ep'), may hold values from 0.05 to 1
- w_gate: bfloat16 [8, 3072, 3072], P('ep', None, 'tp'), may hold values from -0.3125 to 0.3125
- w_up: bfloat16 [8, 3072, 3072], P('ep', None, 'tp'), may hold values from -0.3125 to 0.3125
- w_down: bfloat16 [8, 3072, 3072], P('ep', 'tp'), may hold values from -0.01953125 to 0.01953125
Outputs:
- mixed: bfloat16 [192, 3072], P('ep', 'tp')
Inputs may be any that keep to these rules, and one draw needn't show every extreme that they name: `routing`: each row names 4 different experts. Within the rows of one device (aligned blocks of 24 rows) no expert is named by more than 13 rows, a bound that some block reaches.
All inputs are finite; a program needn't handle non-finite values.
Results may differ from a plain program's by a relative error of at most 0.019.
Values may be sent and summed in bfloat16 or wider, within the bound.
No kernel may reach another device: no remote copies, remote signals or barrier semaphores. Data moves between devices by JAX's collectives and lax.ppermute only.
A program may use at most 64 MiB of HBM per device.

v0:
```python
import jax
import jax.numpy as jnp
from jax import lax
from jax.sharding import PartitionSpec as P

NORM_EPS = 1e-06
CLAMP_LIMIT = 7.0
SIGMOID_SCALE = 1.702


def slot_index(route_rows, expert_total, capacity):
    flat_ids = route_rows.reshape(-1)
    one_hot = (flat_ids[:, None] == jnp.arange(expert_total, dtype=jnp.int32)[None, :]).astype(
        jnp.int32
    )
    before = jnp.cumsum(one_hot, axis=0) - one_hot
    ranked = jnp.sum(before * one_hot, axis=1)
    return flat_ids * capacity + ranked


def local(tokens, norm_gain, routing, route_weight, w_gate, w_up, w_down):
    tok_count = tokens.shape[0]
    width = tokens.shape[1]
    top_count = routing.shape[1]
    expert_total = lax.axis_size("ep") * w_gate.shape[0]
    capacity = max(2, tok_count * top_count // expert_total + 1)
    slice_width = width // lax.axis_size("tp")
    values = tokens.astype(jnp.float32)
    scaled = values * lax.rsqrt(jnp.mean(values * values, axis=-1, keepdims=True) + NORM_EPS)
    normal = (scaled * norm_gain).astype(jnp.bfloat16)
    dest = slot_index(routing, expert_total, capacity)
    slot_ids = jnp.arange(expert_total * capacity, dtype=jnp.int32)
    select = jnp.sum(dest.reshape(1, tok_count, top_count) == slot_ids[:, None, None], axis=2)
    sending = jnp.dot(
        select.astype(jnp.bfloat16), normal, preferred_element_type=jnp.float32
    ).astype(jnp.bfloat16)
    gate_mat = w_gate[0]
    up_mat = w_up[0]
    down_mat = w_down[0]
    own_share = lax.dynamic_slice_in_dim(
        sending, lax.axis_index("tp") * slice_width, slice_width, 1
    )
    arrived = lax.all_to_all(own_share, "ep", split_axis=0, concat_axis=0, tiled=True)
    pieces = lax.all_gather(arrived, "tp", axis=1, tiled=True)
    gate_pre = jnp.dot(pieces, gate_mat, preferred_element_type=jnp.float32)
    up_pre = jnp.dot(pieces, up_mat, preferred_element_type=jnp.float32)
    gated = jnp.minimum(gate_pre, CLAMP_LIMIT)
    upper = jnp.clip(up_pre, -CLAMP_LIMIT, CLAMP_LIMIT)
    hidden = ((upper + 1.0) * gated * jax.nn.sigmoid(SIGMOID_SCALE * gated)).astype(jnp.bfloat16)
    summed = lax.psum_scatter(
        lax.dot_general(
            down_mat, hidden, (((0,), (1,)), ((), ())), preferred_element_type=jnp.float32
        ).astype(jnp.bfloat16),
        "tp",
        scatter_dimension=0,
        tiled=True,
    )
    back = lax.all_to_all(summed, "ep", split_axis=1, concat_axis=1, tiled=True)
    picked = back[:, dest].reshape(slice_width, tok_count, top_count)
    mixed = jnp.sum(picked.astype(jnp.float32) * route_weight[None, :, :], axis=2)
    return mixed.T.astype(jnp.bfloat16)


def solution(mesh):
    placed = (
        P("ep", None),
        P(),
        P("ep", None),
        P("ep", None),
        P("ep", None, "tp"),
        P("ep", None, "tp"),
        P("ep", "tp", None),
    )
    return jax.shard_map(
        local, mesh=mesh, in_specs=placed, out_specs=P("ep", "tp"), check_vma=False
    )
```

profile of v0, /device:TPU:0, one launch (start us, length us, event | category | flops | bytes accessed | tf_op | source)
XLA Modules:
  0.0 87.3 jit_solution(828306079801427838)
XLA Ops:
  6.5 0.0 reduce-scatter.2.cloned.1.call-start
  6.5 0.8 copy.14
  7.3 0.1 eq.28
  7.4 0.1 fusion.48
  7.5 0.1 reduce_window_sum.11
  7.6 0.2 select_reduce_fusion
  7.8 0.1 reduce_sum.41
  7.9 0.1 copy.16
  8.0 0.1 convert_reduce_fusion
  8.1 1.0 %fusion.37 = f32[24]{0:T(128)S(1)} fusion(bf16[24,3072]{1,0:T(8,128)(2,1)} %param.7), kind=kLoop, calls=%fused_computation.23 | loop fusion | flops 221160 | bytes 147552 | tf_op jit(solution)/shard_map/reduce_sum | solution.py:29
  9.2 1.3 %fusion.44 = bf16[104,3072]{1,0:T(8,128)(2,1)S(1)} fusion(bf16[24,3072]{1,0:T(8,128)(2,1)} %param.7, f32[3072]{0:T(1024)} %param.8, f32[24]{0:T(128)S(1)} %add_rsqrt_fusion, s32[104,24]{0,1:T(8,128)S(1)} %convert_reduce_fusion), kind=kOutput, calls=%fused_computation.32 | convolution fusion | flops 15632832 | bytes 808800 | tf_op jit(solution)/shard_map/dot_general | solution.py:34
  10.5 0.1 all_to_all.16
  10.6 15.0 %all_to_all.24 = bf16[8,13,768]{2,1,0:T(8,128)(2,1)S(1)} all-to-all(bf16[8,13,768]{2,1,0:T(8,128)(2,1)S(1)} %all_to_all.16), channel_id=1, replica_groups=mesh['ep'=8,'tp'=4] {'ep'}, dimensions={0} | all-to-all | bytes 319488 | tf_op jit(solution)/shard_map/all_to_all | solution.py:43
  25.6 0.1 all_to_all.18
  25.7 7.8 %all_gather.3 = bf16[104,3072]{1,0:T(8,128)(2,1)S(1)} all-gather(bf16[104,768]{1,0:T(8,128)(2,1)S(1)} %all_to_all.18), channel_id=1, replica_groups=mesh['ep'=8,'tp'=4] {'tp'}, dimensions={1}, use_global_device_ids=true | all-gather | bytes 798720 | tf_op jit(solution)/shard_map/all_gather | solution.py:44
  33.5 3.2 %fusion.12 = f32[104,768]{1,0:T(8,128)S(1)} fusion(bf16[104,3072]{1,0:T(8,128)(2,1)S(1)} %all_gather.3, bf16[1,3072,768]{2,1,0:T(8,128)(2,1)} %param.11), kind=kOutput, calls=%fused_computation.9 | convolution fusion | flops 490813440 | bytes 5677056 | tf_op jit(solution)/shard_map/dot_general | solution.py:45
  36.7 0.0 copy-start
  36.7 6.5 %fusion.9 = bf16[3072,104]{0,1:T(8,128)(2,1)} fusion(bf16[1,768,3072]{2,1,0:T(8,128)(2,1)} %param.13, f32[104,768]{1,0:T(8,128)S(1)} %fusion.12, bf16[104,3072]{1,0:T(8,128)(2,1)S(1)} %all_gather.3, bf16[1,3072,768]{2,1,0:T(8,128)(2,1)} %param.12), kind=kOutput, calls=%fused_computation.8 | convolution fusion | flops 982505472 | bytes 11034624 | tf_op jit(solution)/shard_map/dot_general | solution.py:51
  43.2 0.0 reduce-scatter.2.cloned.1.call-update
  43.2 0.1 mul.76
  43.3 0.0 copy-done
  43.4 0.1 copy.17
  43.4 20.2 %reduce-scatter.2.cloned.1.call-done = bf16[768,104]{0,1:T(8,128)(2,1)} async-done(((bf16[3072,104]{0,1:T(8,128)(2,1)}), bf16[768,104]{0,1:T(8,128)(2,1)}) %reduce-scatter.2.cloned.1.call-update) | async-done | bytes 159760 | tf_op jit(solution)/shard_map/reduce_scatter | solution.py:50
  63.7 1.6 %all_to_all.19 = bf16[768,8,13]{0,2,1:T(8,128)(2,1)} reshape(bf16[768,104]{0,1:T(8,128)(2,1)} %reduce-scatter.2.cloned.1.call-done) | data formatting | bytes 319488 | tf_op jit(solution)/shard_map/all_to_all | solution.py:58
  65.3 5.5 %all-to-all-start.1 = ((bf16[768,8,13]{0,2,1:T(8,128)(2,1)}), bf16[768,8,13]{0,2,1:T(8,128)(2,1)S(1)}, u32[]{:S(2)}, u32[]{:S(2)}) async-start(bf16[768,8,13]{0,2,1:T(8,128)(2,1)} %all_to_all.19), calls=%async_computation.2 | async-start | bytes 393216 | tf_op jit(solution)/shard_map/all_to_all | solution.py:58
  70.8 7.8 %all-to-all-done.1 = bf16[768,8,13]{0,2,1:T(8,128)(2,1)S(1)} async-done(((bf16[768,8,13]{0,2,1:T(8,128)(2,1)}), bf16[768,8,13]{0,2,1:T(8,128)(2,1)S(1)}, u32[]{:S(2)}, u32[]{:S(2)}) %all-to-all-start.1) | async-done | bytes 159776 | tf_op jit(solution)/shard_map/all_to_all | solution.py:58
  78.6 0.1 all_to_all.21
  78.7 0.8 gather_fusion
  79.5 0.1 reshape.54
  79.6 0.9 multiply_reduce_fusion
  (6 shorter events, 0.1 us)
Async XLA Ops:
  6.5 57.1 %reduce-scatter.2.cloned.1.call-start = ((), (), s32[]{:S(2)}) async-start(), calls=%async_computation.3 | async-start | bytes 798720 | tf_op jit(solution)/shard_map/reduce_scatter | solution.py:50
  36.7 6.7 %copy-start = (f32[24,4]{0,1:T(4,128)S(1)}, f32[24,4]{0,1:T(4,128)}, u32[]{:S(2)}) copy-start(f32[24,4]{0,1:T(4,128)} %param.10) | copy-start | bytes 1156
  65.3 13.3 %all-to-all-start.1 = ((bf16[768,8,13]{0,2,1:T(8,128)(2,1)}), bf16[768,8,13]{0,2,1:T(8,128)(2,1)S(1)}, u32[]{:S(2)}, u32[]{:S(2)}) async-start(bf16[768,8,13]{0,2,1:T(8,128)(2,1)} %all_to_all.19), calls=%async_computation.2 | async-start | bytes 393216 | tf_op jit(solution)/shard_map/all_to_all | solution.py:58
Sparse Core Ops, SparseCore 0:
  43.4 20.2 reduce-scatter.1
where the time goes:
time: 87.7 us; the launch traced here: 87.3 us
  waiting for transfers between devices  28 us (32%)
  blocking collectives  22.9 us (26%)
  between operations  13.5 us (15%)
  matrix products  11 us (13%)
  starting transfers between devices  5.5 us (6%)
  local copies, waits for them, and re-layouts  3.96 us (5%)
  other arithmetic  2.44 us (3%)
    reduce_scatter x1, waiting for transfers between devices, local(): lax.psum_scatter(lax.dot_general(down_mat, hidden, (((0,), (1,)), ((), ()...  20.2 us
    all_to_all x1, blocking collectives, local(): lax.all_to_all(own_share, 'ep', split_axis=0, concat_axis=0, tiled=True)  15 us
    all_gather x1, blocking collectives, local(): pieces = lax.all_gather(arrived, 'tp', axis=1, tiled=True)  7.82 us
    all_to_all x1, waiting for transfers between devices, local(): back = lax.all_to_all(summed, 'ep', split_axis=1, concat_axis=1, tiled=True)  7.77 us
    dot_general x1, matrix products, local(): lax.dot_general(down_mat, hidden, (((0,), (1,)), ((), ())), preferred_ele...  6.54 us
    all_to_all x1, starting transfers between devices, local(): back = lax.all_to_all(summed, 'ep', split_axis=1, concat_axis=1, tiled=True)  5.5 us
    dot_general x1, matrix products, local(): gate_pre = jnp.dot(pieces, gate_mat, preferred_element_type=jnp.float32)  3.18 us
  transfers between devices with their start and end apart: 2, of which 2 were waited for; matrix products, arithmetic and copies ran while one was open for 0% of the time, Pallas kernels for 0%

commit v1 on v0

--- a/solution.py
+++ b/solution.py
@@ -41,7 +41,12 @@
         sending, lax.axis_index("tp") * slice_width, slice_width, 1
     )
     arrived = lax.all_to_all(own_share, "ep", split_axis=0, concat_axis=0, tiled=True)
-    pieces = lax.all_gather(arrived, "tp", axis=1, tiled=True)
+    ring = [arrived]
+    for hop in range(3):
+        ring.append(lax.ppermute(ring[-1], "tp", [(dev, (dev + 1) % 4) for dev in range(4)]))
+    pieces = jnp.roll(
+        jnp.concatenate(ring[::-1], axis=1), (lax.axis_index("tp") + 1) * ring[0].shape[1], axis=1
+    )
     gate_pre = jnp.dot(pieces, gate_mat, preferred_element_type=jnp.float32)
     up_pre = jnp.dot(pieces, up_mat, preferred_element_type=jnp.float32)
     gated = jnp.minimum(gate_pre, CLAMP_LIMIT)

time: 87.7 us -> 95 us (1.083)
  waiting for transfers between devices: 28 us -> 42.7 us
  blocking collectives: 22.9 us -> 15 us
    ppermute x0 -> x3, waiting for transfers between devices: none -> 14.1 us  [local(): lax.ppermute(ring[-1], 'tp', [(dev, (dev + 1) % 4) for dev in range(4)])]
    all_gather x1 -> x0, blocking collectives: 7.82 us -> none  [local(): pieces = lax.all_gather(arrived, 'tp', axis=1, tiled=True)]
  transfers between devices with their start and end apart: 2 -> 5, of which waited for: 2 -> 5; matrix products, arithmetic and copies ran while one was open for 0% -> 0% of each run, Pallas kernels for 0% -> 0%
where the time goes in v1:
time: 95 us; the launch traced here: 94.6 us
  waiting for transfers between devices  42.7 us (45%)
  blocking collectives  15 us (16%)
  between operations  13.6 us (14%)
  matrix products  11.2 us (12%)
  starting transfers between devices  5.59 us (6%)
  local copies, waits for them, and re-layouts  4.07 us (4%)
  other arithmetic  2.44 us (3%)
    reduce_scatter x1, waiting for transfers between devices, local(): lax.psum_scatter(lax.dot_general(down_mat, hidden, (((0,), (1,)), ((), ()...  20.9 us
    all_to_all x1, blocking collectives, local(): lax.all_to_all(own_share, 'ep', split_axis=0, concat_axis=0, tiled=True)  15 us
    ppermute x3, waiting for transfers between devices, local(): lax.ppermute(ring[-1], 'tp', [(dev, (dev + 1) % 4) for dev in range(4)])  14.1 us
    all_to_all x1, waiting for transfers between devices, local(): back = lax.all_to_all(summed, 'ep', split_axis=1, concat_axis=1, tiled=True)  7.77 us
    dot_general x1, matrix products, local(): lax.dot_general(down_mat, hidden, (((0,), (1,)), ((), ())), preferred_ele...  6.61 us
    all_to_all x1, starting transfers between devices, local(): back = lax.all_to_all(summed, 'ep', split_axis=1, concat_axis=1, tiled=True)  5.53 us
    dot_general x1, matrix products, local(): gate_pre = jnp.dot(pieces, gate_mat, preferred_element_type=jnp.float32)  3.26 us
  transfers between devices with their start and end apart: 5, of which 5 were waited for; matrix products, arithmetic and copies ran while one was open for 0% of the time, Pallas kernels for 0%

profile of v1, /device:TPU:0, one launch (start us, length us, event | category | flops | bytes accessed | tf_op | source)
XLA Modules:
  0.0 94.6 jit_solution(184464557569465970)
XLA Ops:
  6.5 0.0 reduce-scatter.2.cloned.1.call-start
  6.5 0.8 copy.14
  7.3 0.1 eq.31
  7.4 0.1 fusion.51
  7.5 0.1 reduce_window_sum.11
  7.6 0.2 select_reduce_fusion
  7.8 0.1 reduce_sum.41
  7.9 0.1 copy.16
  8.0 0.1 convert_reduce_fusion
  8.1 1.0 %fusion.40 = f32[24]{0:T(128)S(1)} fusion(bf16[24,3072]{1,0:T(8,128)(2,1)} %param.7), kind=kLoop, calls=%fused_computation.25 | loop fusion | flops 221160 | bytes 147552 | tf_op jit(solution)/shard_map/reduce_sum | solution.py:29
  9.2 1.3 %fusion.47 = bf16[104,3072]{1,0:T(8,128)(2,1)S(1)} fusion(bf16[24,3072]{1,0:T(8,128)(2,1)} %param.7, f32[3072]{0:T(1024)} %param.8, f32[24]{0:T(128)S(1)} %add_rsqrt_fusion, s32[104,24]{0,1:T(8,128)S(1)} %convert_reduce_fusion), kind=kOutput, calls=%fused_computation.34 | convolution fusion | flops 15632832 | bytes 808800 | tf_op jit(solution)/shard_map/dot_general | solution.py:34
  10.5 0.1 all_to_all.16
  10.6 15.0 %all_to_all.24 = bf16[8,13,768]{2,1,0:T(8,128)(2,1)S(1)} all-to-all(bf16[8,13,768]{2,1,0:T(8,128)(2,1)S(1)} %all_to_all.16), channel_id=1, replica_groups=mesh['ep'=8,'tp'=4] {'ep'}, dimensions={0} | all-to-all | bytes 319488 | tf_op jit(solution)/shard_map/all_to_all | solution.py:43
  25.6 0.1 all_to_all.18
  25.7 0.1 collective-permute-start
  25.7 4.7 %collective-permute-done = bf16[104,768]{1,0:T(8,128)(2,1)S(1)} collective-permute-done((bf16[104,768]{1,0:T(8,128)(2,1)S(1)}, bf16[104,768]{1,0:T(8,128)(2,1)S(1)}, u32[]{:S(2)}, u32[]{:S(2)}) %collective-permute-start) | collective-permute-done | bytes 159776 | tf_op jit(solution)/shard_map/ppermute | solution.py:46
  30.4 0.0 collective-permute-start.1
  30.4 4.7 %collective-permute-done.1 = bf16[104,768]{1,0:T(8,128)(2,1)S(1)} collective-permute-done((bf16[104,768]{1,0:T(8,128)(2,1)S(1)}, bf16[104,768]{1,0:T(8,128)(2,1)S(1)}, u32[]{:S(2)}, u32[]{:S(2)}) %collective-permute-start.1) | collective-permute-done | bytes 159776 | tf_op jit(solution)/shard_map/ppermute | solution.py:46
  35.1 0.0 collective-permute-start.2
  35.1 4.7 %collective-permute-done.2 = bf16[104,768]{1,0:T(8,128)(2,1)S(1)} collective-permute-done((bf16[104,768]{1,0:T(8,128)(2,1)S(1)}, bf16[104,768]{1,0:T(8,128)(2,1)S(1)}, u32[]{:S(2)}, u32[]{:S(2)}) %collective-permute-start.2) | collective-permute-done | bytes 159776 | tf_op jit(solution)/shard_map/ppermute | solution.py:46
  40.0 3.3 %fusion.12 = f32[104,768]{1,0:T(8,128)S(1)} fusion(bf16[1,3072,768]{2,1,0:T(8,128)(2,1)} %param.11, bf16[104,6144]{1,0:T(8,128)(2,1)S(1)} %constant_dynamic-update-slice_fusion, s32[]{:T(128)S(6)} %select_n.28), kind=kOutput, calls=%fused_computation.9 | convolution fusion | flops 490813440 | bytes 5677060 | tf_op jit(solution)/shard_map/dot_general | solution.py:50
  43.2 0.0 copy-start
  43.3 6.6 %fusion.9 = bf16[3072,104]{0,1:T(8,128)(2,1)} fusion(bf16[1,768,3072]{2,1,0:T(8,128)(2,1)} %param.13, f32[104,768]{1,0:T(8,128)S(1)} %fusion.12, bf16[1,3072,768]{2,1,0:T(8,128)(2,1)} %param.12, bf16[104,6144]{1,0:T(8,128)(2,1)S(1)} %constant_dynamic-update-slice_fusion, s32[]{:T(128)S(6)} %select_n.28), kind=kOutput, calls=%fused_computation.8 | convolution fusion | flops 982505472 | bytes 11034628 | tf_op jit(solution)/shard_map/dot_general | solution.py:56
  49.9 0.0 reduce-scatter.2.cloned.1.call-update
  49.9 0.1 mul.80
  50.0 0.0 copy-done
  50.0 0.1 copy.17
  50.1 20.9 %reduce-scatter.2.cloned.1.call-done = bf16[768,104]{0,1:T(8,128)(2,1)} async-done(((bf16[3072,104]{0,1:T(8,128)(2,1)}), bf16[768,104]{0,1:T(8,128)(2,1)}) %reduce-scatter.2.cloned.1.call-update) | async-done | bytes 159760 | tf_op jit(solution)/shard_map/reduce_scatter | solution.py:55
  71.0 1.6 %all_to_all.19 = bf16[768,8,13]{0,2,1:T(8,128)(2,1)} reshape(bf16[768,104]{0,1:T(8,128)(2,1)} %reduce-scatter.2.cloned.1.call-done) | data formatting | bytes 319488 | tf_op jit(solution)/shard_map/all_to_all | solution.py:63
  72.6 5.5 %all-to-all-start.1 = ((bf16[768,8,13]{0,2,1:T(8,128)(2,1)}), bf16[768,8,13]{0,2,1:T(8,128)(2,1)S(1)}, u32[]{:S(2)}, u32[]{:S(2)}) async-start(bf16[768,8,13]{0,2,1:T(8,128)(2,1)} %all_to_all.19), calls=%async_computation.2 | async-start | bytes 393216 | tf_op jit(solution)/shard_map/all_to_all | solution.py:63
  78.2 7.8 %all-to-all-done.1 = bf16[768,8,13]{0,2,1:T(8,128)(2,1)S(1)} async-done(((bf16[768,8,13]{0,2,1:T(8,128)(2,1)}), bf16[768,8,13]{0,2,1:T(8,128)(2,1)S(1)}, u32[]{:S(2)}, u32[]{:S(2)}) %all-to-all-start.1) | async-done | bytes 159776 | tf_op jit(solution)/shard_map/all_to_all | solution.py:63
  85.9 0.1 all_to_all.21
  86.0 0.8 gather_fusion
  86.8 0.1 reshape.54
  86.9 0.9 multiply_reduce_fusion
  (14 shorter events, 0.2 us)
Async XLA Ops:
  6.5 64.4 %reduce-scatter.2.cloned.1.call-start = ((), (), s32[]{:S(2)}) async-start(), calls=%async_computation.3 | async-start | bytes 798720 | tf_op jit(solution)/shard_map/reduce_scatter | solution.py:55
  25.7 4.8 %collective-permute-start = (bf16[104,768]{1,0:T(8,128)(2,1)S(1)}, bf16[104,768]{1,0:T(8,128)(2,1)S(1)}, u32[]{:S(2)}, u32[]{:S(2)}) collective-permute-start(bf16[104,768]{1,0:T(8,128)(2,1)S(1)} %all_to_all.18), channel_id=1, source_target_pairs={{0,1},{1,2},{2,3},{3,0},{4,5},{5,6},{6,7},{7,4},{8,9},{9,10},{10,1... | collective-permute-start | bytes 479240 | tf_op jit(solution)/shard_map/ppermute | solution.py:46
  30.4 4.7 %collective-permute-start.1 = (bf16[104,768]{1,0:T(8,128)(2,1)S(1)}, bf16[104,768]{1,0:T(8,128)(2,1)S(1)}, u32[]{:S(2)}, u32[]{:S(2)}) collective-permute-start(bf16[104,768]{1,0:T(8,128)(2,1)S(1)} %collective-permute-done), channel_id=1, source_target_pairs={{0,1},{1,2},{2,3},{3,0},{4,5},{5,6},{6,7},{7,4},{8,9},{9,10},{10,1... | collective-permute-start | bytes 479240 | tf_op jit(solution)/shard_map/ppermute | solution.py:46
  35.1 4.7 %collective-permute-start.2 = (bf16[104,768]{1,0:T(8,128)(2,1)S(1)}, bf16[104,768]{1,0:T(8,128)(2,1)S(1)}, u32[]{:S(2)}, u32[]{:S(2)}) collective-permute-start(bf16[104,768]{1,0:T(8,128)(2,1)S(1)} %collective-permute-done.1), channel_id=1, source_target_pairs={{0,1},{1,2},{2,3},{3,0},{4,5},{5,6},{6,7},{7,4},{8,9},{9,10},{10,1... | collective-permute-start | bytes 479240 | tf_op jit(solution)/shard_map/ppermute | solution.py:46
  43.2 6.7 %copy-start = (f32[24,4]{0,1:T(4,128)S(1)}, f32[24,4]{0,1:T(4,128)}, u32[]{:S(2)}) copy-start(f32[24,4]{0,1:T(4,128)} %param.10) | copy-start | bytes 1156
  72.6 13.3 %all-to-all-start.1 = ((bf16[768,8,13]{0,2,1:T(8,128)(2,1)}), bf16[768,8,13]{0,2,1:T(8,128)(2,1)S(1)}, u32[]{:S(2)}, u32[]{:S(2)}) async-start(bf16[768,8,13]{0,2,1:T(8,128)(2,1)} %all_to_all.19), calls=%async_computation.2 | async-start | bytes 393216 | tf_op jit(solution)/shard_map/all_to_all | solution.py:63
Sparse Core Ops, SparseCore 0:
  50.0 20.9 reduce-scatter.1
